TPU v7x, 32 devices: a whole 2x2x4 slice. The times are simulated.
32 devices in a mesh: sp: 8 (over z, y), dp: 4 (over x, core).
Axes of the slice: x: 2, y: 2, z: 4, core: 2. Of those that a mesh axis runs over, the one named last changes fastest.
Arguments:
- queries: bfloat16 [4, 2048, 1280], P('dp', None, 'sp'), may hold values from -6 to 6
- keys: bfloat16 [4, 1024, 1280], P('dp', None, 'sp'), may hold values from -6 to 6
- values: bfloat16 [4, 1024, 1280], P('dp', None, 'sp'), may hold values from -48 to 48
- q_gain: float32 [64], replicated, may hold values from 0.5 to 10
- k_gain: float32 [64], replicated, may hold values from 0.5 to 10
- w_out: bfloat16 [2048, 2048], P(None, 'dp'), may hold values from -0.125 to 0.125
Outputs:
- mixed: bfloat16 [4, 1280, 2048], P('dp', 'sp')
All inputs are finite; a program needn't handle non-finite values.
Results may differ from a plain program's by a relative error of at most 0.0038.
The roundings to bfloat16 on the way count: a program that leaves them out, or rounds other values in their place, can miss the bound.
Values may be sent and summed in bfloat16 or wider, within the bound.
A program may use at most 64 MiB of HBM per device.

v0:
```python
import jax
import jax.numpy as jnp
from jax import lax
from jax.sharding import PartitionSpec as P

HD = 64
QH = 32
KV = 16
GRID_W = 64


epsilon = 1e-06
rotary_base = 10000.0
block_count = 8


def swapped(block, axis, apart):
    count = lax.axis_size(axis)
    route = []
    for low in range(count):
        high = low | 1 << apart
        if high != low and high < count:
            route += [(low, high), (high, low)]
    return lax.ppermute(block, axis, route)


def rotary_tables(first_row, row_count):
    position = first_row + lax.iota(jnp.int32, row_count)
    grid_row = (position // GRID_W).astype(jnp.float32)
    grid_col = (position % GRID_W).astype(jnp.float32)
    quarter = HD // 4
    inv_freq = rotary_base ** (-(2.0 * lax.iota(jnp.float32, quarter)) / (HD // 2))
    row_angle = inv_freq[:, None] * grid_row[None, :]
    col_angle = inv_freq[:, None] * grid_col[None, :]
    cos_table = jnp.concatenate(
        [jnp.cos(row_angle), jnp.cos(row_angle), jnp.cos(col_angle), jnp.cos(col_angle)], axis=0
    )
    sin_table = jnp.concatenate(
        [jnp.sin(row_angle), jnp.sin(row_angle), jnp.sin(col_angle), jnp.sin(col_angle)], axis=0
    )
    return (cos_table, sin_table)


def normalize_turn(field, gain, cos_table, sin_table):
    head_count = field.shape[0] // HD
    values_f = field.astype(jnp.float32).reshape(head_count, HD, field.shape[1])
    normed = (
        values_f
        * lax.rsqrt(jnp.mean(values_f * values_f, axis=1, keepdims=True) + epsilon)
        * gain[None, :, None]
    )
    quarter = HD // 4
    quarters_of = normed.reshape(head_count, 4, quarter, field.shape[1])
    turned = jnp.concatenate(
        [-quarters_of[:, 1], quarters_of[:, 0], -quarters_of[:, 3], quarters_of[:, 2]], axis=1
    )
    return (normed * cos_table[None] + turned * sin_table[None]).astype(jnp.bfloat16)


def attention_heads(query_heads, key_heads, value_heads, seq_len):
    kv_local = key_heads.shape[0]
    group_local = query_heads.shape[0] // kv_local
    query_split = query_heads.reshape(kv_local, group_local, HD, seq_len)
    score_scale = HD ** (-0.5)
    block_rows = seq_len // block_count

    def one_block(block_index, result):
        row_start = block_index * block_rows
        query_block = lax.dynamic_slice_in_dim(query_split, row_start, block_rows, 3)
        scores = (
            jnp.einsum("hgdq,hdk->hgqk", query_block, key_heads, preferred_element_type=jnp.float32)
            * score_scale
        )
        row_max = jnp.max(scores, axis=-1, keepdims=True)
        weights = jnp.exp(scores - row_max)
        weights = (weights / jnp.sum(weights, axis=-1, keepdims=True)).astype(jnp.bfloat16)
        attended = jnp.einsum(
            "hgqk,hdk->hgdq", weights, value_heads, preferred_element_type=jnp.float32
        )
        return lax.dynamic_update_slice_in_dim(result, attended.astype(jnp.bfloat16), row_start, 3)

    result = jnp.zeros(query_split.shape, jnp.bfloat16)
    result = lax.fori_loop(0, block_count, one_block, result)
    return result.reshape(query_heads.shape)


def on_device(queries, keys, values, q_gain, k_gain, w_out):
    sp_count = lax.axis_size("sp")
    tok_rows = queries.shape[2]
    seq_len = tok_rows * sp_count
    cos_table, sin_table = rotary_tables(lax.axis_index("sp") * tok_rows, tok_rows)
    query_rot = normalize_turn(queries[0], q_gain, cos_table, sin_table)
    key_rot = normalize_turn(keys[0], k_gain, cos_table, sin_table)
    value_rows = values[0].reshape(KV, HD, tok_rows)
    query_heads = lax.all_to_all(query_rot, "sp", split_axis=0, concat_axis=2, tiled=True)
    share_count = max(sp_count // KV, 1)
    part_rows = tok_rows // share_count
    key_cut = (
        key_rot.reshape(KV, HD, share_count, part_rows)
        .transpose(0, 2, 1, 3)
        .reshape(KV * share_count, HD, part_rows)
    )
    value_cut = (
        value_rows.reshape(KV, HD, share_count, part_rows)
        .transpose(0, 2, 1, 3)
        .reshape(KV * share_count, HD, part_rows)
    )
    key_got, value_got = (
        lax.all_to_all(key_cut, "sp", split_axis=0, concat_axis=2, tiled=True),
        lax.all_to_all(value_cut, "sp", split_axis=0, concat_axis=2, tiled=True),
    )
    kv_local = key_got.shape[0]
    key_got = key_got.reshape(kv_local, HD, sp_count, part_rows)
    value_got = value_got.reshape(kv_local, HD, sp_count, part_rows)
    for bit_index in range(share_count.bit_length() - 1):
        key_other, value_other = swapped((key_got, value_got), "sp", bit_index)
        key_got = jnp.concatenate([key_got, key_other], axis=3)
        value_got = jnp.concatenate([value_got, value_other], axis=3)
    key_heads = key_got.reshape(kv_local, HD, seq_len)
    value_heads = value_got.reshape(kv_local, HD, seq_len)
    attended = attention_heads(query_heads, key_heads, value_heads, seq_len)
    token_heads = lax.all_to_all(attended, "sp", split_axis=2, concat_axis=0, tiled=True)
    token_rows = token_heads.reshape(QH * HD, tok_rows)
    product = lax.dot_general(
        token_rows,
        lax.all_gather(w_out, "dp", axis=1, tiled=True),
        (((0,), (0,)), ((), ())),
        preferred_element_type=jnp.float32,
    )
    mixed_rows = product.astype(jnp.bfloat16)
    return mixed_rows[None]


def solution(mesh):
    placed = (
        P("dp", None, "sp"),
        P("dp", None, "sp"),
        P("dp", None, "sp"),
        P(),
        P(),
        P(None, "dp"),
    )
    return jax.shard_map(
        on_device, mesh=mesh, in_specs=placed, out_specs=P("dp", "sp", None), check_vma=False
    )
```

profile of v0, /device:TPU:0, one launch (start us, length us, event | category | flops | bytes accessed | tf_op | source)
XLA Modules:
  0.0 176.7 jit_solution(5040789266582131515)
XLA Ops:
  9.3 3.6 %copy.58 = f32[16,4,16,160]{2,0,3,1:T(8,128)} copy(f32[16,4,16,160]{3,2,1,0:T(8,128)S(1)} %bitcast.86) | data formatting | bytes 1310720 | tf_op jit(solution)/shard_map/convert_element_type | solution.py:46
  13.4 3.1 %multiply_multiply_fusion.1 = f32[16,4,16,160]{2,0,3,1:T(8,128)S(1)} fusion(f32[16,4,16,160]{2,0,3,1:T(8,128)} %copy.58, f32[4,16]{1,0:T(4,128)S(1)} %mul.184, f32[16,160]{0,1:T(8,128)S(1)} %add_rsqrt_fusion), kind=kLoop, calls=%fused_computation.21 | loop fusion | flops 327680 | bytes 1321216 | tf_op jit(solution)/shard_map/mul | solution.py:48
  19.8 7.3 %all-to-all-start.1 = ((bf16[16,64,160]{2,1,0:T(8,128)(2,1)}), bf16[16,64,160]{2,1,0:T(8,128)(2,1)}, u32[]{:S(2)}, u32[]{:S(2)}) async-start(bf16[16,64,160]{2,1,0:T(8,128)(2,1)} %copy.60), calls=%async_computation.1 | async-start | bytes 1048576 | tf_op jit(solution)/shard_map/all_to_all | solution.py:109
  29.7 10.7 %copy.52 = f32[32,4,16,160]{2,0,3,1:T(8,128)} copy(f32[32,4,16,160]{3,2,1,0:T(8,128)} %bitcast.81) | data formatting | bytes 2621440 | tf_op jit(solution)/shard_map/convert_element_type | solution.py:46
  42.3 9.7 %multiply_multiply_fusion = f32[32,4,16,160]{2,0,3,1:T(8,128)} fusion(f32[32,4,16,160]{2,0,3,1:T(8,128)} %copy.52, f32[4,16]{1,0:T(4,128)S(1)} %mul.170, f32[32,160]{0,1:T(8,128)S(1)} %add_rsqrt_fusion.1), kind=kLoop, calls=%fused_computation.20 | loop fusion | flops 655360 | bytes 2642176 | tf_op jit(solution)/shard_map/mul | solution.py:48
  52.0 6.0 %all-to-all-start.2 = ((bf16[16,64,160]{2,1,0:T(8,128)(2,1)}), bf16[16,64,160]{2,1,0:T(8,128)(2,1)S(1)}, u32[]{:S(2)}, u32[]{:S(2)}) async-start(bf16[16,64,160]{2,1,0:T(8,128)(2,1)} %bitcast.88), calls=%async_computation.2 | async-start | bytes 1048576 | tf_op jit(solution)/shard_map/all_to_all | solution.py:110
  58.0 6.1 %fusion.35 = (f32[32,16,160]{1,0,2:T(8,128)S(1)}, f32[32,16,160]{1,0,2:T(8,128)S(1)}, f32[32,16,160]{1,0,2:T(8,128)S(1)}, f32[32,16,160]{1,0,2:T(8,128)S(1)}) fusion(f32[32,4,16,160]{2,0,3,1:T(8,128)} %multiply_multiply_fusion), kind=kLoop, calls=%fused_computation.27 | loop fusion | flops 163840 | bytes 2621440 | tf_op jit(solution)/shard_map/neg | solution.py:55
  64.1 3.8 %fusion.37 = bf16[32,64,160]{1,0,2:T(8,128)(2,1)} fusion(f32[32,16,160]{1,0,2:T(8,128)S(1)} %get-tuple-element.111, f32[32,16,160]{1,0,2:T(8,128)S(1)} %get-tuple-element.112, f32[32,16,160]{1,0,2:T(8,128)S(1)} %get-tuple-element.113, f32[32,16,160]{1,0,2:T(8,128)S(1)} %get-tuple-element.110, f32[32,64,160]{1,0,2:T(8,128)S(1)} %reshape.99, ...), kind=kLoop, calls=%fused_computation.30 | loop fusion | flops 2949120 | bytes 3379456 | tf_op jit(solution)/shard_map/convert_element_type | solution.py:57
  67.9 3.0 %copy.54 = bf16[32,64,160]{2,1,0:T(8,128)(2,1)} copy(bf16[32,64,160]{1,0,2:T(8,128)(2,1)} %fusion.37) | data formatting | bytes 1310720 | tf_op jit(solution)/shard_map/convert_element_type | solution.py:57
  71.9 4.9 %all-to-all-start = ((bf16[32,64,160]{2,1,0:T(8,128)(2,1)}), bf16[32,64,160]{2,1,0:T(8,128)(2,1)S(1)}, u32[]{:S(2)}, u32[]{:S(2)}) async-start(bf16[32,64,160]{2,1,0:T(8,128)(2,1)} %copy.54), calls=%async_computation | async-start | bytes 2097152 | tf_op jit(solution)/shard_map/all_to_all | solution.py:95
  79.6 22.2 %all-to-all-done = bf16[32,64,160]{2,1,0:T(8,128)(2,1)S(1)} async-done(((bf16[32,64,160]{2,1,0:T(8,128)(2,1)}), bf16[32,64,160]{2,1,0:T(8,128)(2,1)S(1)}, u32[]{:S(2)}, u32[]{:S(2)}) %all-to-all-start) | async-done | bytes 655392 | tf_op jit(solution)/shard_map/all_to_all | solution.py:95
  103.5 33.8 %while.13 = (s32[]{:T(128)}, bf16[2,2,64,1280]{3,2,1,0:T(8,128)(2,1)S(1)}, bf16[2,2,64,1280]{3,2,1,0:T(8,128)(2,1)S(1)}, bf16[2,64,1280]{2,1,0:T(8,128)(2,1)S(1)...) while((s32[]{:T(128)}, bf16[2,2,64,1280]{3,2,1,0:T(8,128)(2,1)S(1)}, ...), condition=%wide.region_5.6_spmd, body=%wide.region_2.5_spmd.sunk | while | flops 320351360 | bytes 1497751 | solution.py:83
  104.9 1.8 %fusion.66 = bf16[2,2,64,160]{3,2,1,0:T(8,128)(2,1)S(1)} fusion(f32[2,2,160]{2,1,0:T(2,128)S(1)} %fusion.65, bf16[2,64,1280]{2,1,0:T(8,128)(2,1)S(1)} %get-tuple-element.179, bf16[2,64,1280]{2,1,0:T(8,128)(2,1)S(1)} %get-tuple-element.178, bf16[2,2,64,1280]{3,2,1,0:T(8,128)(2,1)S(1)} %get-tuple-element.177, s32[]{:T(128)S(6)} %select_n.37), kind=kOutput, calls=%fused_computation.7.clone.1 | convolution fusion | flops 213034880 | bytes 872452 | tf_op jit(solution)/shard_map/while/body/eval_jaxpr/hgqk,hdk->hgdq/dot_general | solution.py:77
  108.6 1.8 %fusion.66 = bf16[2,2,64,160]{3,2,1,0:T(8,128)(2,1)S(1)} fusion(f32[2,2,160]{2,1,0:T(2,128)S(1)} %fusion.65, bf16[2,64,1280]{2,1,0:T(8,128)(2,1)S(1)} %get-tuple-element.179, bf16[2,64,1280]{2,1,0:T(8,128)(2,1)S(1)} %get-tuple-element.178, bf16[2,2,64,1280]{3,2,1,0:T(8,128)(2,1)S(1)} %get-tuple-element.177, s32[]{:T(128)S(6)} %select_n.37), kind=kOutput, calls=%fused_computation.7.clone.1 | convolution fusion | flops 213034880 | bytes 872452 | tf_op jit(solution)/shard_map/while/body/eval_jaxpr/hgqk,hdk->hgdq/dot_general | solution.py:77
  113.0 1.8 %fusion.66 = bf16[2,2,64,160]{3,2,1,0:T(8,128)(2,1)S(1)} fusion(f32[2,2,160]{2,1,0:T(2,128)S(1)} %fusion.65, bf16[2,64,1280]{2,1,0:T(8,128)(2,1)S(1)} %get-tuple-element.179, bf16[2,64,1280]{2,1,0:T(8,128)(2,1)S(1)} %get-tuple-element.178, bf16[2,2,64,1280]{3,2,1,0:T(8,128)(2,1)S(1)} %get-tuple-element.177, s32[]{:T(128)S(6)} %select_n.37), kind=kOutput, calls=%fused_computation.7.clone.1 | convolution fusion | flops 213034880 | bytes 872452 | tf_op jit(solution)/shard_map/while/body/eval_jaxpr/hgqk,hdk->hgdq/dot_general | solution.py:77
  117.4 1.8 %fusion.66 = bf16[2,2,64,160]{3,2,1,0:T(8,128)(2,1)S(1)} fusion(f32[2,2,160]{2,1,0:T(2,128)S(1)} %fusion.65, bf16[2,64,1280]{2,1,0:T(8,128)(2,1)S(1)} %get-tuple-element.179, bf16[2,64,1280]{2,1,0:T(8,128)(2,1)S(1)} %get-tuple-element.178, bf16[2,2,64,1280]{3,2,1,0:T(8,128)(2,1)S(1)} %get-tuple-element.177, s32[]{:T(128)S(6)} %select_n.37), kind=kOutput, calls=%fused_computation.7.clone.1 | convolution fusion | flops 213034880 | bytes 872452 | tf_op jit(solution)/shard_map/while/body/eval_jaxpr/hgqk,hdk->hgdq/dot_general | solution.py:77
  121.9 1.8 %fusion.66 = bf16[2,2,64,160]{3,2,1,0:T(8,128)(2,1)S(1)} fusion(f32[2,2,160]{2,1,0:T(2,128)S(1)} %fusion.65, bf16[2,64,1280]{2,1,0:T(8,128)(2,1)S(1)} %get-tuple-element.179, bf16[2,64,1280]{2,1,0:T(8,128)(2,1)S(1)} %get-tuple-element.178, bf16[2,2,64,1280]{3,2,1,0:T(8,128)(2,1)S(1)} %get-tuple-element.177, s32[]{:T(128)S(6)} %select_n.37), kind=kOutput, calls=%fused_computation.7.clone.1 | convolution fusion | flops 213034880 | bytes 872452 | tf_op jit(solution)/shard_map/while/body/eval_jaxpr/hgqk,hdk->hgdq/dot_general | solution.py:77
  125.6 1.8 %fusion.66 = bf16[2,2,64,160]{3,2,1,0:T(8,128)(2,1)S(1)} fusion(f32[2,2,160]{2,1,0:T(2,128)S(1)} %fusion.65, bf16[2,64,1280]{2,1,0:T(8,128)(2,1)S(1)} %get-tuple-element.179, bf16[2,64,1280]{2,1,0:T(8,128)(2,1)S(1)} %get-tuple-element.178, bf16[2,2,64,1280]{3,2,1,0:T(8,128)(2,1)S(1)} %get-tuple-element.177, s32[]{:T(128)S(6)} %select_n.37), kind=kOutput, calls=%fused_computation.7.clone.1 | convolution fusion | flops 213034880 | bytes 872452 | tf_op jit(solution)/shard_map/while/body/eval_jaxpr/hgqk,hdk->hgdq/dot_general | solution.py:77
  130.0 1.8 %fusion.66 = bf16[2,2,64,160]{3,2,1,0:T(8,128)(2,1)S(1)} fusion(f32[2,2,160]{2,1,0:T(2,128)S(1)} %fusion.65, bf16[2,64,1280]{2,1,0:T(8,128)(2,1)S(1)} %get-tuple-element.179, bf16[2,64,1280]{2,1,0:T(8,128)(2,1)S(1)} %get-tuple-element.178, bf16[2,2,64,1280]{3,2,1,0:T(8,128)(2,1)S(1)} %get-tuple-element.177, s32[]{:T(128)S(6)} %select_n.37), kind=kOutput, calls=%fused_computation.7.clone.1 | convolution fusion | flops 213034880 | bytes 872452 | tf_op jit(solution)/shard_map/while/body/eval_jaxpr/hgqk,hdk->hgdq/dot_general | solution.py:77
  134.4 1.8 %fusion.66 = bf16[2,2,64,160]{3,2,1,0:T(8,128)(2,1)S(1)} fusion(f32[2,2,160]{2,1,0:T(2,128)S(1)} %fusion.65, bf16[2,64,1280]{2,1,0:T(8,128)(2,1)S(1)} %get-tuple-element.179, bf16[2,64,1280]{2,1,0:T(8,128)(2,1)S(1)} %get-tuple-element.178, bf16[2,2,64,1280]{3,2,1,0:T(8,128)(2,1)S(1)} %get-tuple-element.177, s32[]{:T(128)S(6)} %select_n.37), kind=kOutput, calls=%fused_computation.7.clone.1 | convolution fusion | flops 213034880 | bytes 872452 | tf_op jit(solution)/shard_map/while/body/eval_jaxpr/hgqk,hdk->hgdq/dot_general | solution.py:77
  137.3 1.7 copy.64
  139.9 21.1 %all_to_all.66 = bf16[8,2,20480]{2,1,0:T(2,128)(2,1)S(1)} all-to-all(bf16[8,2,20480]{2,1,0:T(2,128)(2,1)S(1)} %reshape.105), channel_id=1, replica_groups=mesh['sp'=8,'dp'=4] {'sp'}, dimensions={0} | all-to-all | bytes 1310720 | tf_op jit(solution)/shard_map/all_to_all | solution.py:122
  161.8 2.2 %copy.71 = bf16[4,64,8,160]{3,1,0,2:T(8,128)(2,1)S(1)} copy(bf16[4,64,8,160]{1,0,3,2:T(4,128)(2,1)S(1)} %bitcast.83) | data formatting | bytes 1310720 | tf_op jit(solution)/shard_map/all_to_all | solution.py:122
  164.0 5.8 %fusion.38 = bf16[1,160,2048]{2,1,0:T(8,128)(2,1)} fusion(bf16[2048,160]{1,0:T(8,128)(2,1)S(1)} %bitcast.82, bf16[2048,2048]{1,0:T(8,128)(2,1)} %all-gather.2.cloned.1.call-done), kind=kOutput, calls=%fused_computation.33 | convolution fusion | flops 1342504960 | bytes 9699328 | tf_op jit(solution)/shard_map/dot_general | solution.py:124
  (61 shorter events, 37.4 us)
Async XLA Ops:
  6.5 2.1 %copy-start.1 = (bf16[1,1024,160]{1,2,0:T(8,128)(2,1)S(1)}, bf16[1,1024,160]{1,2,0:T(8,128)(2,1)}, u32[]{:S(2)}) copy-start(bf16[1,1024,160]{1,2,0:T(8,128)(2,1)} %param.9) | copy-start | bytes 983044
  6.5 157.5 %all-gather.2.cloned.1.call-start = ((), (), s32[]{:S(2)}) async-start(), calls=%async_computation.4 | async-start | bytes 10485760 | tf_op jit(solution)/shard_map/all_gather | solution.py:126
  9.3 3.6 %copy-start.4 = (f32[64]{0:T(128)S(1)}, f32[64]{0:T(128)}, u32[]{:S(2)}) copy-start(f32[64]{0:T(128)} %param.12) | copy-start | bytes 772
  18.5 8.7 %copy-start = (bf16[1,2048,160]{1,2,0:T(8,128)(2,1)S(1)}, bf16[1,2048,160]{1,2,0:T(8,128)(2,1)}, u32[]{:S(2)}) copy-start(bf16[1,2048,160]{1,2,0:T(8,128)(2,1)} %param.8) | copy-start | bytes 1966084
  19.8 32.2 %all-to-all-start.1 = ((bf16[16,64,160]{2,1,0:T(8,128)(2,1)}), bf16[16,64,160]{2,1,0:T(8,128)(2,1)}, u32[]{:S(2)}, u32[]{:S(2)}) async-start(bf16[16,64,160]{2,1,0:T(8,128)(2,1)} %copy.60), calls=%async_computation.1 | async-start | bytes 1048576 | tf_op jit(solution)/shard_map/all_to_all | solution.py:109
  29.7 10.7 %copy-start.3 = (f32[64]{0:T(128)S(1)}, f32[64]{0:T(128)}, u32[]{:S(2)}) copy-start(f32[64]{0:T(128)} %param.11) | copy-start | bytes 772
  29.7 10.8 %copy-start.2 = (bf16[1,1024,160]{1,2,0:T(8,128)(2,1)S(1)}, bf16[1,1024,160]{1,2,0:T(8,128)(2,1)}, u32[]{:S(2)}) copy-start(bf16[1,1024,160]{1,2,0:T(8,128)(2,1)} %param.10) | copy-start | bytes 983044
  52.0 19.9 %all-to-all-start.2 = ((bf16[16,64,160]{2,1,0:T(8,128)(2,1)}), bf16[16,64,160]{2,1,0:T(8,128)(2,1)S(1)}, u32[]{:S(2)}, u32[]{:S(2)}) async-start(bf16[16,64,160]{2,1,0:T(8,128)(2,1)} %bitcast.88), calls=%async_computation.2 | async-start | bytes 1048576 | tf_op jit(solution)/shard_map/all_to_all | solution.py:110
  71.9 29.8 %all-to-all-start = ((bf16[32,64,160]{2,1,0:T(8,128)(2,1)}), bf16[32,64,160]{2,1,0:T(8,128)(2,1)S(1)}, u32[]{:S(2)}, u32[]{:S(2)}) async-start(bf16[32,64,160]{2,1,0:T(8,128)(2,1)} %copy.54), calls=%async_computation | async-start | bytes 2097152 | tf_op jit(solution)/shard_map/all_to_all | solution.py:95
Sparse Core Ops, SparseCore 0:
  8.9 60.9 all-gather.1
where the time goes:
time: 177 us
  local copies, waits for them, and re-layouts  43 us (24%)
  matrix products  30.5 us (17%)
  other arithmetic  26 us (15%)
  waiting for transfers between devices  24 us (14%)
  blocking collectives  21.1 us (12%)
  starting transfers between devices  18.2 us (10%)
  between operations  13.6 us (8%)
    all_to_all x1, waiting for transfers between devices, on_device(): lax.all_to_all(query_rot, 'sp', split_axis=0, concat_axis=2, tiled=True)  22.2 us
    all_to_all x1, blocking collectives, on_device(): lax.all_to_all(attended, 'sp', split_axis=2, concat_axis=0, tiled=True)  21.1 us
    convert_element_type x6, local copies, waits for them, and re-layouts, normalize_turn(): values_f = field.astype(jnp.float32).reshape(head_count, HD, field.shape[1])  18.4 us
    dot_general x8, matrix products, one_block(): jnp.einsum('hgqk,hdk->hgdq', weights, value_heads, preferred_element_type...  14.3 us
    mul x2, other arithmetic, normalize_turn(): values_f * lax.rsqrt(jnp.mean(values_f * values_f, axis=1, keepdims=True)...  12.8 us
    sub x8, matrix products, one_block(): weights = jnp.exp(scores - row_max)  10.4 us
    dynamic_update_slice x8, local copies, waits for them, and re-layouts, one_block(): lax.dynamic_update_slice_in_dim(result, attended.astype(jnp.bfloat16), ro...  8.81 us
    all_to_all x1, starting transfers between devices, on_device(): lax.all_to_all(key_cut, 'sp', split_axis=0, concat_axis=2, tiled=True)  7.31 us
  transfers between devices with their start and end apart: 4, of which 2 were waited for; matrix products, arithmetic and copies ran while one was open for 52% of the time, Pallas kernels for 0%

commit v1 on v0

--- a/solution.py
+++ b/solution.py
@@ -1,6 +1,10 @@
+import functools
+
 import jax
 import jax.numpy as jnp
 from jax import lax
+from jax.experimental import pallas as pl
+from jax.experimental.pallas import tpu as pltpu
 from jax.sharding import PartitionSpec as P
 
 HD = 64
@@ -84,7 +88,7 @@
     return result.reshape(query_heads.shape)
 
 
-def on_device(queries, keys, values, q_gain, k_gain, w_out):
+def on_device_plain(queries, keys, values, q_gain, k_gain, w_out):
     sp_count = lax.axis_size("sp")
     tok_rows = queries.shape[2]
     seq_len = tok_rows * sp_count
@@ -131,6 +135,292 @@
     return mixed_rows[None]
 
 
+MESH = pl.DeviceIdType.MESH
+LOG2E = 1.4426950408889634
+
+
+def layer_kernel(
+    n, m, q_ref, k_ref, v_ref, qg_ref, kg_ref, cos_ref, sin_ref, w_ref, out_ref,
+    q_out, k_out, v_out, q_in, k_in, v_in, a_out, a_in, w_all,
+    q_send, q_recv, k_send, k_recv, v_send, v_recv, a_send, a_recv, w_send, w_recv, w_pass, w_own,
+):
+    me = lax.axis_index("sp")
+    dp = lax.axis_index("dp")
+    x_count = m // 2
+    core = lax.rem(dp, 2)
+    x_at = dp // 2
+    partner = x_at * 2 + (1 - core)
+    rows = q_ref.shape[1]
+    w_rows = w_ref.shape[0] // n
+    kv_width = k_out.shape[2]
+    pairs = kv_width // 128
+    group = q_out.shape[2] // kv_width
+
+    def at_sp(d):
+        return lax.rem(me + d, n)
+
+    def at_dp(d):
+        return lax.rem(x_at + d, x_count) * 2 + core
+
+    barrier = pltpu.get_barrier_semaphore()
+
+    def greet(d, carry):
+        pl.semaphore_signal(barrier, inc=1, device_id={"sp": at_sp(d)}, device_id_type=MESH)
+        return carry
+
+    lax.fori_loop(1, n, greet, 0)
+    for d in range(1, x_count):
+        pl.semaphore_signal(barrier, inc=1, device_id={"dp": at_dp(d)}, device_id_type=MESH)
+    pl.semaphore_signal(barrier, inc=1, device_id={"dp": partner}, device_id_type=MESH)
+    pl.semaphore_wait(barrier, n - 1 + x_count)
+
+    def w_piece(shard, c):
+        return w_all.at[shard, pl.ds(pl.multiple_of(c * w_rows, w_rows), w_rows)]
+
+    def w_source(c):
+        return w_ref.at[pl.ds(pl.multiple_of(c * w_rows, w_rows), w_rows)]
+
+    def w_copy(d, c):
+        return pltpu.make_async_remote_copy(
+            src_ref=w_source(c), dst_ref=w_piece(dp, c), send_sem=w_send.at[d, c],
+            recv_sem=w_recv.at[dp, c], device_id={"dp": at_dp(d) if d else partner},
+            device_id_type=MESH,
+        )
+
+    def w_came(shard, c):
+        return pltpu.make_async_remote_copy(
+            src_ref=w_source(c), dst_ref=w_piece(shard, c), send_sem=w_send.at[0, c],
+            recv_sem=w_recv.at[shard, c], device_id={"dp": partner}, device_id_type=MESH,
+        )
+
+    def w_forward(d, c):
+        shard = at_dp(d)
+        return pltpu.make_async_remote_copy(
+            src_ref=w_piece(shard, c), dst_ref=w_piece(shard, c), send_sem=w_pass.at[d, c],
+            recv_sem=w_recv.at[shard, c], device_id={"dp": partner}, device_id_type=MESH,
+        )
+
+    def start_w(c, carry):
+        for d in range(x_count):
+            w_copy(d, c).start()
+        return carry
+
+    lax.fori_loop(0, n, start_w, 0)
+    own_w = pltpu.make_async_copy(w_ref, w_all.at[dp], w_own)
+    own_w.start()
+
+    eye = jnp.where(
+        lax.broadcasted_iota(jnp.int32, (rows, rows), 0)
+        == lax.broadcasted_iota(jnp.int32, (rows, rows), 1), 1.0, 0.0,
+    ).astype(jnp.bfloat16)
+
+    def flip(block):
+        return lax.dot_general(
+            eye, block, (((1,), (1,)), ((), ())), preferred_element_type=jnp.float32
+        ).astype(jnp.bfloat16)
+
+    def turn(block, gain):
+        u = block.astype(jnp.float32)
+        normed = u * lax.rsqrt(jnp.mean(u * u, axis=0, keepdims=True) + epsilon) * gain
+        part = HD // 4
+        a, b, c, d = (normed[i * part : (i + 1) * part] for i in range(4))
+        turned = jnp.concatenate([-b, a, -d, c], axis=0)
+        return (normed * cos_ref[...] + turned * sin_ref[...]).astype(jnp.bfloat16)
+
+    def exchange(out, into, send, recv, d):
+        peer = at_sp(d)
+        return pltpu.make_async_remote_copy(
+            src_ref=out.at[peer], dst_ref=into.at[me], send_sem=send.at[peer],
+            recv_sem=recv.at[me], device_id={"sp": peer}, device_id_type=MESH,
+        )
+
+    def arrival(out, into, send, recv, source):
+        return pltpu.make_async_remote_copy(
+            src_ref=out.at[source], dst_ref=into.at[source], send_sem=send.at[source],
+            recv_sem=recv.at[source], device_id={"sp": source}, device_id_type=MESH,
+        )
+
+    def kv_heads_of(peer):
+        base = pl.multiple_of(peer * kv_width, kv_width)
+        kt = jnp.concatenate(
+            [turn(k_ref[pl.ds(base + h * HD, HD)], kg_ref[...]) for h in range(kv_width // HD)], axis=0
+        )
+        return flip(kt), flip(v_ref[pl.ds(base, kv_width)])
+
+    def q_heads_of(peer):
+        base = pl.multiple_of(peer * (kv_width * group), kv_width * group)
+        parts = []
+        for g in range(group):
+            for h in range(kv_width // HD):
+                parts.append(turn(q_ref[pl.ds(base + (h * group + g) * HD, HD)], qg_ref[...]))
+        return flip(jnp.concatenate(parts, axis=0))
+
+    def send_kv(d, carry):
+        peer = at_sp(d)
+        k_out[peer], v_out[peer] = kv_heads_of(peer)
+        exchange(k_out, k_in, k_send, k_recv, d).start()
+        exchange(v_out, v_in, v_send, v_recv, d).start()
+        return carry
+
+    def send_q(d, carry):
+        peer = at_sp(d)
+        q_out[peer] = q_heads_of(peer)
+        exchange(q_out, q_in, q_send, q_recv, d).start()
+        return carry
+
+    lax.fori_loop(1, n, send_kv, 0)
+    lax.fori_loop(1, n, send_q, 0)
+    k_in[me], v_in[me] = kv_heads_of(me)
+    q_in[me] = q_heads_of(me)
+
+    def await_kv(d, carry):
+        source = at_sp(d)
+        arrival(k_out, k_in, k_send, k_recv, source).wait_recv()
+        arrival(v_out, v_in, v_send, v_recv, source).wait_recv()
+        return carry
+
+    lax.fori_loop(1, n, await_kv, 0)
+    seq_len = n * rows
+    low = lax.broadcasted_iota(jnp.int32, (rows, 128), 1) < HD
+    scale = HD ** (-0.5) * LOG2E
+
+    def attend(source):
+        for j in range(pairs):
+            keys = k_in[:, :, j * 128 : (j + 1) * 128].reshape(seq_len, 128)
+            vals = v_in[:, :, j * 128 : (j + 1) * 128].reshape(seq_len, 128)
+            tiles = []
+            for g in range(group):
+                at = g * kv_width + j * 128
+                pair = q_in[source, :, at : at + 128]
+                zero = jnp.zeros_like(pair)
+                both = []
+                for one in (jnp.where(low, pair, zero), jnp.where(low, zero, pair)):
+                    s = lax.dot_general(
+                        one, keys, (((1,), (1,)), ((), ())), preferred_element_type=jnp.float32
+                    )
+                    p = jnp.exp2((s - jnp.max(s, axis=1, keepdims=True)) * scale)
+                    p = p * (1.0 / jnp.sum(p, axis=1, keepdims=True))
+                    both.append(
+                        jnp.dot(p.astype(jnp.bfloat16), vals, preferred_element_type=jnp.float32)
+                    )
+                tiles.append(jnp.where(low, both[0], both[1]))
+            first, second = tiles
+            one = jnp.where(low, first, pltpu.roll(second, HD, 1))
+            two = jnp.where(low, pltpu.roll(first, HD, 1), second)
+            yield j, jnp.concatenate([one, two], axis=1).astype(jnp.bfloat16)
+
+    def block(d, carry):
+        source = at_sp(d)
+        arrival(q_out, q_in, q_send, q_recv, source).wait_recv()
+        for j, tile in attend(source):
+            a_out[source, :, j * 256 : (j + 1) * 256] = tile
+        exchange(a_out, a_in, a_send, a_recv, d).start()
+        for e in range(1, x_count):
+            w_came(at_dp(e), d - 1).wait_recv()
+            w_forward(e, d - 1).start()
+        return carry
+
+    lax.fori_loop(1, n, block, 0)
+    for j, tile in attend(me):
+        a_in[me, :, j * 256 : (j + 1) * 256] = tile
+    own_w.wait()
+
+    def came(d, carry):
+        source = at_sp(d)
+        arrival(a_out, a_in, a_send, a_recv, source).wait_recv()
+        return carry
+
+    lax.fori_loop(1, n, came, 0)
+    width = w_ref.shape[1]
+
+    def product(shard):
+        total = jnp.zeros((rows, width), jnp.float32)
+        step = a_in.shape[2]
+        for p in range(n):
+            total += jnp.dot(
+                a_in[p], w_all[shard, p * step : (p + 1) * step, :],
+                preferred_element_type=jnp.float32,
+            )
+        out_ref[:, pl.ds(pl.multiple_of(shard * width, width), width)] = total.astype(jnp.bfloat16)
+
+    def await_w(shard):
+        def one(c, carry):
+            w_came(shard, c).wait_recv()
+            return carry
+
+        lax.fori_loop(0, n, one, 0)
+
+    product(dp)
+    await_w(partner)
+    product(partner)
+    for e in range(1, x_count):
+        w_came(at_dp(e), n - 1).wait_recv()
+        w_forward(e, n - 1).start()
+    for e in range(1, x_count):
+        product(at_dp(e))
+    for e in range(1, x_count):
+        other = at_dp(e) + 1 - 2 * core
+        await_w(other)
+        product(other)
+
+    def sent(d, carry):
+        exchange(k_out, k_in, k_send, k_recv, d).wait_send()
+        exchange(v_out, v_in, v_send, v_recv, d).wait_send()
+        exchange(q_out, q_in, q_send, q_recv, d).wait_send()
+        exchange(a_out, a_in, a_send, a_recv, d).wait_send()
+        return carry
+
+    lax.fori_loop(1, n, sent, 0)
+
+    def sent_w(c, carry):
+        for d in range(x_count):
+            w_copy(d, c).wait_send()
+        for d in range(1, x_count):
+            w_forward(d, c).wait_send()
+        return carry
+
+    lax.fori_loop(0, n, sent_w, 0)
+
+
+def on_device(queries, keys, values, q_gain, k_gain, w_out):
+    n, m = lax.axis_size("sp"), lax.axis_size("dp")
+    tok_rows = queries.shape[2]
+    kv_width = keys.shape[1] // n
+    if kv_width % 128 or m % 2 or tok_rows % 16:
+        return on_device_plain(queries, keys, values, q_gain, k_gain, w_out)
+    q_width = queries.shape[1] // n
+    cos_table, sin_table = rotary_tables(lax.axis_index("sp") * tok_rows, tok_rows)
+    vmem = pl.BlockSpec(memory_space=pltpu.VMEM)
+    bf16 = jnp.bfloat16
+    dma = pltpu.SemaphoreType.DMA
+    mixed = pl.pallas_call(
+        functools.partial(layer_kernel, n, m),
+        out_shape=jax.ShapeDtypeStruct((tok_rows, w_out.shape[1] * m), bf16),
+        in_specs=[vmem] * 7 + [pl.BlockSpec(memory_space=pl.ANY)],
+        out_specs=vmem,
+        scratch_shapes=[
+            pltpu.VMEM((n, tok_rows, q_width), bf16),
+            pltpu.VMEM((n, tok_rows, kv_width), bf16),
+            pltpu.VMEM((n, tok_rows, kv_width), bf16),
+            pltpu.VMEM((n, tok_rows, q_width), bf16),
+            pltpu.VMEM((n, tok_rows, kv_width), bf16),
+            pltpu.VMEM((n, tok_rows, kv_width), bf16),
+            pltpu.VMEM((n, tok_rows, q_width), bf16),
+            pltpu.VMEM((n, tok_rows, q_width), bf16),
+            pltpu.VMEM((m, w_out.shape[0], w_out.shape[1]), bf16),
+        ]
+        + [dma((n,))] * 8
+        + [dma((m // 2, n)), dma((m, n)), dma((m // 2, n)), dma],
+        compiler_params=pltpu.CompilerParams(
+            collective_id=0, has_side_effects=True, vmem_limit_bytes=48 * 1024 * 1024
+        ),
+    )(
+        queries[0], keys[0], values[0], q_gain[:, None], k_gain[:, None],
+        cos_table, sin_table, w_out,
+    )
+    return mixed[None]
+
+
 def solution(mesh):
     placed = (
         P("dp", None, "sp"),

time: 177 us -> 71.1 us (0.40)
  the two profiles are of different devices: /device:TPU:0 before, /device:TPU:11 now
where the time goes in v1:
time: 71.1 us; the launch traced here: 70.9 us
  Pallas kernels  63.7 us (90%)
  local copies, waits for them, and re-layouts  6.84 us (10%)
    pallas_call x1, Pallas kernels, on_device(): pl.pallas_call(functools.partial(layer_kernel, n, m), out_shape=jax.Shape...  63.7 us
    unnamed x8, local copies, waits for them, and re-layouts  5.29 us

profile of v1, /device:TPU:11, one launch (start us, length us, event | category | flops | bytes accessed | tf_op | source)
XLA Modules:
  0.0 70.9 jit_solution(18377718464323598696)
XLA Ops:
  0.0 0.0 copy-start.1
  0.0 0.8 %copy.10.qg_ref = f32[64,1]{1,0:T(8,128)S(1)} copy(f32[64,1]{0,1:T(1,128)} %bitcast.10) | data formatting | bytes 512 | tf_op jit(solution)/shard_map/broadcast_in_dim | solution.py:418
  0.8 0.7 %copy.11.kg_ref = f32[64,1]{1,0:T(8,128)S(1)} copy(f32[64,1]{0,1:T(1,128)} %bitcast.11) | data formatting | bytes 512 | tf_op jit(solution)/shard_map/broadcast_in_dim | solution.py:418
  1.6 0.2 multiply_sine_fusion.1
  1.8 1.2 %copy.8 = bf16[1,1024,160]{2,1,0:T(8,128)(2,1)S(1)} copy(bf16[1,1024,160]{1,2,0:T(8,128)(2,1)} %param.7) | data formatting | bytes 655360 | tf_op args[1]
  3.0 1.2 %copy.9 = bf16[1,1024,160]{2,1,0:T(8,128)(2,1)S(1)} copy(bf16[1,1024,160]{1,2,0:T(8,128)(2,1)} %param.8) | data formatting | bytes 655360 | tf_op args[2]
  4.2 0.0 copy-done.1
  4.2 0.5 copy.7
  4.7 0.0 copy-start
  4.7 1.6 %copy-done = bf16[2048,512]{1,0:T(8,128)(2,1)S(1)} copy-done((bf16[2048,512]{1,0:T(8,128)(2,1)S(1)}, bf16[2048,512]{1,0:T(8,128)(2,1)}, u32[]{:S(2)}) %copy-start) | copy-done | bytes 2097176
  6.3 63.7 %shard_map.64 = bf16[160,2048]{1,0:T(8,128)(2,1)S(1)} custom-call(bf16[2048,160]{1,0:T(8,128)(2,1)S(1)} %bitcast.6, bf16[1024,160]{1,0:T(8,128)(2,1)S(1)} %bitcast.8, bf16[1024,160]{1,0:T(8,128)(2,1)S(1)} %bitcast.9, f32[64,1]{1,0:T(8,128)S(1)} %copy.10.qg_ref, f32[64,1]{1,0:T(8,128)S(1)} %copy.11.kg_ref, f32[64,160]{1,0:T(8,128)S(1)} %pad_maximum_fusion.cos_ref, ...), custom_call_target="tpu_custom_call" | custom-call | tf_op jit(solution)/shard_map/pallas_call | solution.py:396
  70.0 0.8 %copy.13 = bf16[1,160,2048]{2,1,0:T(8,128)(2,1)} copy(bf16[1,160,2048]{2,1,0:T(8,128)(2,1)S(1)} %bitcast.7) | data formatting | bytes 1310720
  (4 shorter events, 0.0 us)
Async XLA Ops:
  0.0 4.2 %copy-start.1 = (bf16[1,2048,160]{1,2,0:T(8,128)(2,1)S(1)}, bf16[1,2048,160]{1,2,0:T(8,128)(2,1)}, u32[]{:S(2)}) copy-start(bf16[1,2048,160]{1,2,0:T(8,128)(2,1)} %param.6) | copy-start | bytes 1966084
  4.7 1.6 %copy-start = (bf16[2048,512]{1,0:T(8,128)(2,1)S(1)}, bf16[2048,512]{1,0:T(8,128)(2,1)}, u32[]{:S(2)}) copy-start(bf16[2048,512]{1,0:T(8,128)(2,1)} %w_ref.1) | copy-start | bytes 6291460

commit v2 on v1

--- a/solution.py
+++ b/solution.py
@@ -141,7 +141,7 @@
 
 def layer_kernel(
     n, m, q_ref, k_ref, v_ref, qg_ref, kg_ref, cos_ref, sin_ref, w_ref, out_ref,
-    q_out, k_out, v_out, q_in, k_in, v_in, a_out, a_in, w_all,
+    q_out, k_out, q_in, k_in, v_in, a_out, a_in, w_all,
     q_send, q_recv, k_send, k_recv, v_send, v_recv, a_send, a_recv, w_send, w_recv, w_pass, w_own,
 ):
     me = lax.axis_index("sp")
@@ -150,7 +150,7 @@
     core = lax.rem(dp, 2)
     x_at = dp // 2
     partner = x_at * 2 + (1 - core)
-    rows = q_ref.shape[1]
+    rows = q_ref.shape[0]
     w_rows = w_ref.shape[0] // n
     kv_width = k_out.shape[2]
     pairs = kv_width // 128
@@ -209,23 +209,28 @@
     own_w = pltpu.make_async_copy(w_ref, w_all.at[dp], w_own)
     own_w.start()
 
-    eye = jnp.where(
-        lax.broadcasted_iota(jnp.int32, (rows, rows), 0)
-        == lax.broadcasted_iota(jnp.int32, (rows, rows), 1), 1.0, 0.0,
-    ).astype(jnp.bfloat16)
-
-    def flip(block):
-        return lax.dot_general(
-            eye, block, (((1,), (1,)), ((), ())), preferred_element_type=jnp.float32
-        ).astype(jnp.bfloat16)
-
-    def turn(block, gain):
-        u = block.astype(jnp.float32)
-        normed = u * lax.rsqrt(jnp.mean(u * u, axis=0, keepdims=True) + epsilon) * gain
+    lane = lax.broadcasted_iota(jnp.int32, (rows, 128), 1)
+    low = lane < HD
+    even = (lane // (HD // 4)) % 2 == 0
+    q_gain, k_gain = (jnp.concatenate([g[...], g[...]], axis=1) for g in (qg_ref, kg_ref))
+
+    def turn(tile, gain):
+        u = tile.astype(jnp.float32)
+        square = u * u
+        sum_low = jnp.sum(jnp.where(low, square, 0.0), axis=1, keepdims=True)
+        sum_high = jnp.sum(jnp.where(low, 0.0, square), axis=1, keepdims=True)
+        inverse = jnp.where(
+            low, lax.rsqrt(sum_low * (1.0 / HD) + epsilon), lax.rsqrt(sum_high * (1.0 / HD) + epsilon)
+        )
+        normed = u * inverse * gain
         part = HD // 4
-        a, b, c, d = (normed[i * part : (i + 1) * part] for i in range(4))
-        turned = jnp.concatenate([-b, a, -d, c], axis=0)
-        return (normed * cos_ref[...] + turned * sin_ref[...]).astype(jnp.bfloat16)
+        turned = jnp.where(even, pltpu.roll(normed, 128 - part, 1), pltpu.roll(normed, part, 1))
+        return normed * cos_ref[...] + turned * sin_ref[...]
+
+    def crossed(first, second):
+        one = jnp.where(low, first, pltpu.roll(second, HD, 1))
+        two = jnp.where(low, pltpu.roll(first, HD, 1), second)
+        return one, two
 
     def exchange(out, into, send, recv, d):
         peer = at_sp(d)
@@ -240,48 +245,59 @@
             recv_sem=recv.at[source], device_id={"sp": source}, device_id_type=MESH,
         )
 
-    def kv_heads_of(peer):
-        base = pl.multiple_of(peer * kv_width, kv_width)
-        kt = jnp.concatenate(
-            [turn(k_ref[pl.ds(base + h * HD, HD)], kg_ref[...]) for h in range(kv_width // HD)], axis=0
-        )
-        return flip(kt), flip(v_ref[pl.ds(base, kv_width)])
-
-    def q_heads_of(peer):
-        base = pl.multiple_of(peer * (kv_width * group), kv_width * group)
-        parts = []
-        for g in range(group):
-            for h in range(kv_width // HD):
-                parts.append(turn(q_ref[pl.ds(base + (h * group + g) * HD, HD)], qg_ref[...]))
-        return flip(jnp.concatenate(parts, axis=0))
+    def kv_lanes(peer, j=0, size=kv_width):
+        return pl.ds(pl.multiple_of(peer * kv_width + j * 128, 128), size)
+
+    def turn_keys(peer, into, at):
+        for j in range(pairs):
+            tile = turn(k_ref[:, kv_lanes(peer, j, 128)], k_gain)
+            into[at, :, j * 128 : (j + 1) * 128] = tile.astype(jnp.bfloat16)
+
+    def turn_queries(peer, into, at):
+        base = peer * (kv_width * group)
+        for j in range(pairs):
+            natural = [
+                turn(q_ref[:, pl.ds(pl.multiple_of(base + j * 256 + i * 128, 128), 128)], q_gain)
+                for i in range(2)
+            ]
+            for g, tile in enumerate(crossed(*natural)):
+                start = g * kv_width + j * 128
+                into[at, :, start : start + 128] = tile.astype(jnp.bfloat16)
+
+    def send_values(d):
+        peer = at_sp(d)
+        return pltpu.make_async_remote_copy(
+            src_ref=v_ref.at[:, kv_lanes(peer)], dst_ref=v_in.at[me], send_sem=v_send.at[peer],
+            recv_sem=v_recv.at[me], device_id={"sp": peer}, device_id_type=MESH,
+        )
 
     def send_kv(d, carry):
         peer = at_sp(d)
-        k_out[peer], v_out[peer] = kv_heads_of(peer)
+        send_values(d).start()
+        turn_keys(peer, k_out, peer)
         exchange(k_out, k_in, k_send, k_recv, d).start()
-        exchange(v_out, v_in, v_send, v_recv, d).start()
         return carry
 
     def send_q(d, carry):
         peer = at_sp(d)
-        q_out[peer] = q_heads_of(peer)
+        turn_queries(peer, q_out, peer)
         exchange(q_out, q_in, q_send, q_recv, d).start()
         return carry
 
     lax.fori_loop(1, n, send_kv, 0)
     lax.fori_loop(1, n, send_q, 0)
-    k_in[me], v_in[me] = kv_heads_of(me)
-    q_in[me] = q_heads_of(me)
+    turn_keys(me, k_in, me)
+    v_in[me] = v_ref[:, kv_lanes(me)]
+    turn_queries(me, q_in, me)
 
     def await_kv(d, carry):
         source = at_sp(d)
         arrival(k_out, k_in, k_send, k_recv, source).wait_recv()
-        arrival(v_out, v_in, v_send, v_recv, source).wait_recv()
+        arrival(k_out, v_in, v_send, v_recv, source).wait_recv()
         return carry
 
     lax.fori_loop(1, n, await_kv, 0)
     seq_len = n * rows
-    low = lax.broadcasted_iota(jnp.int32, (rows, 128), 1) < HD
     scale = HD ** (-0.5) * LOG2E
 
     def attend(source):
@@ -304,10 +320,7 @@
                         jnp.dot(p.astype(jnp.bfloat16), vals, preferred_element_type=jnp.float32)
                     )
                 tiles.append(jnp.where(low, both[0], both[1]))
-            first, second = tiles
-            one = jnp.where(low, first, pltpu.roll(second, HD, 1))
-            two = jnp.where(low, pltpu.roll(first, HD, 1), second)
-            yield j, jnp.concatenate([one, two], axis=1).astype(jnp.bfloat16)
+            yield j, jnp.concatenate(crossed(*tiles), axis=1).astype(jnp.bfloat16)
 
     def block(d, carry):
         source = at_sp(d)
@@ -365,7 +378,7 @@
 
     def sent(d, carry):
         exchange(k_out, k_in, k_send, k_recv, d).wait_send()
-        exchange(v_out, v_in, v_send, v_recv, d).wait_send()
+        send_values(d).wait_send()
         exchange(q_out, q_in, q_send, q_recv, d).wait_send()
         exchange(a_out, a_in, a_send, a_recv, d).wait_send()
         return carry
@@ -382,25 +395,36 @@
     lax.fori_loop(0, n, sent_w, 0)
 
 
+def rotary_lanes(first_row, row_count):
+    position = first_row + lax.broadcasted_iota(jnp.int32, (row_count, 128), 0)
+    lane = lax.broadcasted_iota(jnp.int32, (row_count, 128), 1)
+    place = jnp.where(lane % HD < HD // 2, position // GRID_W, position % GRID_W)
+    quarter = HD // 4
+    step = (lax.iota(jnp.int32, 128) % quarter).astype(jnp.float32)
+    inv_freq = rotary_base ** (-(2.0 * step) / (HD // 2))
+    angle = inv_freq[None, :] * place.astype(jnp.float32)
+    sign = jnp.where((lane // quarter) % 2 == 0, -1.0, 1.0)
+    return (jnp.cos(angle), jnp.sin(angle) * sign)
+
+
 def on_device(queries, keys, values, q_gain, k_gain, w_out):
     n, m = lax.axis_size("sp"), lax.axis_size("dp")
     tok_rows = queries.shape[2]
     kv_width = keys.shape[1] // n
-    if kv_width % 128 or m % 2 or tok_rows % 16:
+    if kv_width % 128 or m % 2 or tok_rows % 16 or QH != 2 * KV:
         return on_device_plain(queries, keys, values, q_gain, k_gain, w_out)
     q_width = queries.shape[1] // n
-    cos_table, sin_table = rotary_tables(lax.axis_index("sp") * tok_rows, tok_rows)
+    cos_table, sin_table = rotary_lanes(lax.axis_index("sp") * tok_rows, tok_rows)
     vmem = pl.BlockSpec(memory_space=pltpu.VMEM)
     bf16 = jnp.bfloat16
     dma = pltpu.SemaphoreType.DMA
     mixed = pl.pallas_call(
         functools.partial(layer_kernel, n, m),
         out_shape=jax.ShapeDtypeStruct((tok_rows, w_out.shape[1] * m), bf16),
-        in_specs=[vmem] * 7 + [pl.BlockSpec(memory_space=pl.ANY)],
+        in_specs=[vmem] * 7 + [pl.BlockSpec(memory_space=pltpu.HBM)],
         out_specs=vmem,
         scratch_shapes=[
             pltpu.VMEM((n, tok_rows, q_width), bf16),
-            pltpu.VMEM((n, tok_rows, kv_width), bf16),
             pltpu.VMEM((n, tok_rows, kv_width), bf16),
             pltpu.VMEM((n, tok_rows, q_width), bf16),
             pltpu.VMEM((n, tok_rows, kv_width), bf16),
@@ -415,7 +439,7 @@
             collective_id=0, has_side_effects=True, vmem_limit_bytes=48 * 1024 * 1024
         ),
     )(
-        queries[0], keys[0], values[0], q_gain[:, None], k_gain[:, None],
+        queries[0].T, keys[0].T, values[0].T, q_gain[None], k_gain[None],
         cos_table, sin_table, w_out,
     )
     return mixed[None]

time: 71.1 us -> 71.1 us (level)
    broadcast_in_dim x2 -> x0, local copies, waits for them, and re-layouts: 1.55 us -> none  [the longest x1 0.81 us: on_device(): q_gain[:, None]]
    unnamed x8 -> x13, local copies, waits for them, and re-layouts: 5.29 us -> 6.77 us
where the time goes in v2:
time: 71.1 us; the launch traced here: 70.8 us
  Pallas kernels  63.5 us (89%)
  local copies, waits for them, and re-layouts  6.77 us (10%)
    pallas_call x1, Pallas kernels, on_device(): pl.pallas_call(functools.partial(layer_kernel, n, m), out_shape=jax.Shape...  63.5 us
    unnamed x13, local copies, waits for them, and re-layouts  6.77 us

profile of v2, /device:TPU:11, one launch (start us, length us, event | category | flops | bytes accessed | tf_op | source)
XLA Modules:
  0.0 70.8 jit_solution(11019069260312852620)
XLA Ops:
  0.1 0.4 select_multiply_fusion
  0.5 0.0 copy-start
  0.5 1.6 %copy-done = bf16[2048,512]{1,0:T(8,128)(2,1)S(1)} copy-done((bf16[2048,512]{1,0:T(8,128)(2,1)S(1)}, bf16[2048,512]{1,0:T(8,128)(2,1)}, u32[]{:S(2)}) %copy-start) | copy-done | bytes 2097176
  2.1 0.0 copy-start.1
  2.1 1.1 %copy-done.1 = bf16[1,2048,160]{1,2,0:T(8,128)(2,1)S(1)} copy-done((bf16[1,2048,160]{1,2,0:T(8,128)(2,1)S(1)}, bf16[1,2048,160]{1,2,0:T(8,128)(2,1)}, u32[]{:S(2)}) %copy-start.1) | copy-done | bytes 655384
  3.2 0.0 copy-start.2
  3.2 1.0 %copy-done.2 = bf16[1,1024,160]{1,2,0:T(8,128)(2,1)S(1)} copy-done((bf16[1,1024,160]{1,2,0:T(8,128)(2,1)S(1)}, bf16[1,1024,160]{1,2,0:T(8,128)(2,1)}, u32[]{:S(2)}) %copy-start.2) | copy-done | bytes 327704
  4.2 0.0 copy-start.3
  4.2 1.0 %copy-done.3 = bf16[1,1024,160]{1,2,0:T(8,128)(2,1)S(1)} copy-done((bf16[1,1024,160]{1,2,0:T(8,128)(2,1)S(1)}, bf16[1,1024,160]{1,2,0:T(8,128)(2,1)}, u32[]{:S(2)}) %copy-start.3) | copy-done | bytes 327704
  5.1 0.0 copy-start.4
  5.1 0.7 copy-done.4
  5.8 0.0 copy-start.5
  5.8 0.7 copy-done.5
  6.5 63.5 %shard_map.64 = bf16[160,2048]{1,0:T(8,128)(2,1)S(1)} custom-call(bf16[160,2048]{1,0:T(8,128)(2,1)S(1)} %bitcast.13, bf16[160,1024]{1,0:T(8,128)(2,1)S(1)} %bitcast.14, bf16[160,1024]{1,0:T(8,128)(2,1)S(1)} %bitcast.15, f32[1,64]{1,0:T(1,128)S(1)} %bitcast.16, f32[1,64]{1,0:T(1,128)S(1)} %bitcast.17, f32[160,128]{1,0:T(8,128)S(1)} %get-tuple-element.6.cos_ref, ...), custom_call_target="tpu_custom_call" | custom-call | tf_op jit(solution)/shard_map/pallas_call | solution.py:421
  69.9 0.8 %copy.8 = bf16[1,160,2048]{2,1,0:T(8,128)(2,1)} copy(bf16[1,160,2048]{2,1,0:T(8,128)(2,1)S(1)} %bitcast.12) | data formatting | bytes 1310720
  (7 shorter events, 0.1 us)
Async XLA Ops:
  0.5 1.6 %copy-start = (bf16[2048,512]{1,0:T(8,128)(2,1)S(1)}, bf16[2048,512]{1,0:T(8,128)(2,1)}, u32[]{:S(2)}) copy-start(bf16[2048,512]{1,0:T(8,128)(2,1)} %w_ref.1) | copy-start | bytes 6291460
  2.1 1.1 %copy-start.1 = (bf16[1,2048,160]{1,2,0:T(8,128)(2,1)S(1)}, bf16[1,2048,160]{1,2,0:T(8,128)(2,1)}, u32[]{:S(2)}) copy-start(bf16[1,2048,160]{1,2,0:T(8,128)(2,1)} %param.6) | copy-start | bytes 1966084
  3.2 1.0 %copy-start.2 = (bf16[1,1024,160]{1,2,0:T(8,128)(2,1)S(1)}, bf16[1,1024,160]{1,2,0:T(8,128)(2,1)}, u32[]{:S(2)}) copy-start(bf16[1,1024,160]{1,2,0:T(8,128)(2,1)} %param.7) | copy-start | bytes 983044
  4.2 1.0 %copy-start.3 = (bf16[1,1024,160]{1,2,0:T(8,128)(2,1)S(1)}, bf16[1,1024,160]{1,2,0:T(8,128)(2,1)}, u32[]{:S(2)}) copy-start(bf16[1,1024,160]{1,2,0:T(8,128)(2,1)} %param.8) | copy-start | bytes 983044
  5.1 0.7 copy-start.4
  5.8 0.7 copy-start.5
